TPU v7x, 32 devices: a whole 2x2x4 slice. The times are simulated.
32 devices in a mesh: sp: 8 (over z, y), tp: 4 (over x, core).
Axes of the slice: x: 2, y: 2, z: 4, core: 2. Of those that a mesh axis runs over, the one named last changes fastest.
Arguments:
- queries: bfloat16 [4096, 1024], P('sp', 'tp'), may hold values from -6 to 6
- keys: bfloat16 [4096, 1024], P('sp', 'tp'), may hold values from -6 to 6
- values: bfloat16 [4096, 1024], P('sp', 'tp'), may hold values from -6 to 6
- cum_gate: float32 [4096, 16], P('sp', 'tp'), as said below
- documents: int32 [4096], P('sp'), may hold values from 0 to 3, never falling along the last dimension, each value on 1 to 2048 neighbouring positions
- head_gain: float32 [1024], P('tp'), may hold values from 0.1 to 1.9
- out_weight: bfloat16 [1024, 2048], replicated, may hold values from -0.1875 to 0.1875
- resid: bfloat16 [4096, 2048], P(('sp', 'tp')), may hold values from -6 to 6
- norm_gain: float32 [2048], replicated, may hold values from 0.1 to 1.9
- routes: int32 [4096, 2], P(('sp', 'tp')), may hold values from 0 to 7, all different within a row; in each aligned block of 128 rows (0 to 127, 128 to 255, ...) at most 64 rows name the same one
- route_weights: float32 [4096, 2], P(('sp', 'tp')), may hold values from 0.25 to 1
- w_gate: bfloat16 [8, 2048, 3584], P('sp', None, 'tp'), may hold values from -0.125 to 0.125
- w_up: bfloat16 [8, 2048, 3584], P('sp', None, 'tp'), may hold values from -0.125 to 0.125
- w_down: bfloat16 [8, 3584, 2048], P('sp', 'tp'), may hold values from -0.09375 to 0.09375
Outputs:
- mixed: bfloat16 [4096, 2048], P(('sp', 'tp'))
Inputs may be any that keep to these rules, and one draw needn't show every extreme that they name: `cum_gate`: along the positions each head's values never rise. `documents`: document numbers never fall along the positions. `routes`: the 2 experts of a row differ. In each aligned block of 128 rows no expert is named more than 64 times; in some blocks an expert is named exactly 64 times.
All inputs are finite; a program needn't handle non-finite values.
Results may differ from a plain program's by a relative error of at most 0.015.
Values may be sent and summed in bfloat16 or wider, within the bound.
A program may use at most 128 MiB of HBM per device.

v0:
```python
import math

import jax
import jax.numpy as jnp
from jax import lax
from jax.sharding import PartitionSpec as P

EPS = 1e-06


def on_device(
    queries,
    keys,
    values,
    cum_gate,
    documents,
    head_gain,
    out_weight,
    resid,
    norm_gain,
    routes,
    route_weights,
    w_gate,
    w_up,
    w_down,
):
    tokens = queries.shape[0]
    heads_here = cum_gate.shape[1]
    width_here = queries.shape[1]
    head_size = width_here // heads_here
    score_scale = head_size ** (-0.5)
    first_pos = lax.axis_index("sp") * tokens
    query_pos = first_pos + jnp.arange(tokens, dtype=jnp.int32)
    query_row_block = queries.reshape(tokens, heads_here, head_size)
    history = lax.all_gather(cum_gate, "sp", axis=0, tiled=True)
    initial = (
        jnp.full((tokens, heads_here), -1e30, jnp.float32),
        jnp.zeros((tokens, heads_here), jnp.float32),
        jnp.zeros((tokens, heads_here, head_size), jnp.float32),
    )
    running = initial
    key_part = lax.all_gather(keys, "sp", axis=0, tiled=True)
    value_part = lax.all_gather(values, "sp", axis=0, tiled=True)
    doc_part = lax.all_gather(documents, "sp", axis=0, tiled=True)
    length = key_part.shape[0]
    block_len = math.gcd(length, 512)

    def visit_block(current, step_index):
        offset = step_index * block_len
        key_block = lax.dynamic_slice_in_dim(key_part, offset, block_len, 0).reshape(
            block_len, heads_here, head_size
        )
        value_block = lax.dynamic_slice_in_dim(value_part, offset, block_len, 0).reshape(
            block_len, heads_here, head_size
        )
        doc_block = lax.dynamic_slice_in_dim(doc_part, offset, block_len, 0)
        gate_block = lax.dynamic_slice_in_dim(history, offset, block_len, 0)
        key_pos = offset + jnp.arange(block_len, dtype=jnp.int32)

        def attend(before):
            row_max, row_sum, weighted = before
            scores = (
                jnp.einsum(
                    "qhd,khd->qhk", query_row_block, key_block, preferred_element_type=jnp.float32
                )
                * score_scale
            )
            scores = scores + cum_gate[:, :, None] - gate_block.T[None, :, :]
            allowed = (
                (key_pos[None, :] <= query_pos[:, None])
                & (doc_block[None, :] == documents[:, None])
            )[:, None, :]
            scores = jnp.where(allowed, scores, -1e30)
            next_max = jnp.maximum(row_max, jnp.max(scores, axis=-1))
            unscaled = jnp.where(allowed, jnp.exp(scores - next_max[:, :, None]), 0.0)
            rescale = jnp.exp(row_max - next_max)
            row_sum = row_sum * rescale + jnp.sum(unscaled, axis=-1)
            weighted = weighted * rescale[:, :, None] + jnp.einsum(
                "qhk,khd->qhd",
                unscaled.astype(jnp.bfloat16),
                value_block,
                preferred_element_type=jnp.float32,
            )
            return (next_max, row_sum, weighted)

        skipped = (key_pos[0] > query_pos[-1]) | (doc_block[-1] < documents[0])
        return (lax.cond(skipped, lambda kept: kept, attend, current), None)

    running, unused = lax.scan(
        visit_block, running, jnp.arange(length // block_len, dtype=jnp.int32)
    )
    row_max, row_sum, weighted = running
    attended = weighted / row_sum[:, :, None]
    mean_square = jnp.mean(attended * attended, axis=-1, keepdims=True)
    head_normed = (
        (attended * lax.rsqrt(mean_square + EPS)).reshape(tokens, width_here) * head_gain
    ).astype(jnp.bfloat16)
    tp_count = lax.axis_size("tp")
    local_rows = tokens // tp_count
    regrouped = lax.all_to_all(head_normed, "tp", split_axis=0, concat_axis=1, tiled=True)
    projected = jnp.dot(regrouped, out_weight, preferred_element_type=jnp.float32)
    stream = lax.optimization_barrier((resid.astype(jnp.float32) + projected).astype(jnp.bfloat16))
    widened = stream.astype(jnp.float32)
    mean_wide = jnp.mean(widened * widened, axis=-1, keepdims=True)
    expert_input = (widened * lax.rsqrt(mean_wide + EPS) * norm_gain).astype(jnp.bfloat16)
    top_count = routes.shape[1]
    expert_count = lax.axis_size("sp")
    model_width = stream.shape[1]
    capacity = 2 * top_count * tokens // (tp_count * expert_count)
    flat_routes = routes.reshape(-1)
    route_total = flat_routes.shape[0]
    onehot = (flat_routes[:, None] == jnp.arange(expert_count, dtype=jnp.int32)[None, :]).astype(
        jnp.int32
    )
    ranks = jnp.sum(jnp.cumsum(onehot, axis=0) * onehot, axis=1) - 1
    targets = flat_routes * capacity + ranks
    owners = jnp.arange(route_total, dtype=jnp.int32) // top_count
    slot_owner = jnp.zeros((expert_count * capacity,), jnp.int32).at[targets].set(owners)
    slot_used = jnp.zeros((expert_count * capacity,), jnp.bool_).at[targets].set(True)
    outbound = jnp.where(slot_used[:, None], expert_input[slot_owner], jnp.zeros((), jnp.bfloat16))
    outbound = outbound.reshape(expert_count, capacity, model_width)
    fanned = lax.all_gather(
        lax.all_to_all(outbound, "sp", split_axis=0, concat_axis=0, tiled=True)[:, None],
        "tp",
        axis=1,
        tiled=True,
    )
    flat_rows = fanned.reshape(-1, model_width)
    gate_out = jnp.dot(flat_rows, w_gate[0], preferred_element_type=jnp.float32)
    up_out = jnp.dot(flat_rows, w_up[0], preferred_element_type=jnp.float32)
    hidden = (jax.nn.silu(gate_out) * up_out).astype(jnp.bfloat16)
    partial_value = jnp.dot(hidden, w_down[0], preferred_element_type=jnp.float32)
    partial_value = lax.optimization_barrier(partial_value.astype(jnp.bfloat16)).astype(jnp.float32)
    finish_partial_value = partial_value.reshape(fanned.shape)
    summed = lax.psum_scatter(
        finish_partial_value.astype(jnp.bfloat16), "tp", scatter_dimension=1, tiled=True
    ).astype(jnp.float32)
    returned = lax.all_to_all(
        summed[:, 0].astype(jnp.bfloat16), "sp", split_axis=0, concat_axis=0, tiled=True
    )
    results = returned.reshape(expert_count * capacity, model_width)[targets]
    results = results.reshape(local_rows, top_count, model_width)
    mixed = widened + jnp.sum(route_weights[:, :, None] * results.astype(jnp.float32), axis=1)
    return mixed.astype(jnp.bfloat16)


def solution(mesh):
    in_specs = (
        P("sp", "tp"),
        P("sp", "tp"),
        P("sp", "tp"),
        P("sp", "tp"),
        P("sp"),
        P("tp"),
        P(),
        P(("sp", "tp"), None),
        P(),
        P(("sp", "tp"), None),
        P(("sp", "tp"), None),
        P("sp", None, "tp"),
        P("sp", None, "tp"),
        P("sp", "tp", None),
    )
    out_specs = P(("sp", "tp"), None)
    return jax.shard_map(
        on_device, mesh=mesh, in_specs=in_specs, out_specs=out_specs, check_vma=False
    )
```

profile of v0, /device:TPU:0, one launch (start us, length us, event | category | flops | bytes accessed | tf_op | source)
XLA Modules:
  0.0 586.6 jit_solution(9266547671738930573)
XLA Ops:
  6.5 1.8 copy.38
  8.4 1.8 copy.40
  10.2 0.8 copy.44
  11.3 1.1 copy.39
  12.4 0.6 reduce-window.6
  13.2 0.7 broadcast_multiply_fusion.1
  14.3 1.4 scatter_custom_fusion.1
  15.7 28.1 %all-gather.1 = s32[8,1,512]{2,1,0:T(1,128)S(1)} all-gather(s32[1,1,512]{2,1,0:T(1,128)} %bitcast.84), channel_id=1, replica_groups=mesh['sp'=8,'tp'=4] {'sp'}, dimensions={0}, use_global_device_ids=true | all-gather | bytes 18432 | tf_op jit(solution)/shard_map/all_gather | solution.py:44
  43.8 31.1 %all_gather.17 = f32[4096,4]{0,1:T(4,128)S(1)} all-gather(f32[512,4]{0,1:T(4,128)} %param.21), channel_id=1, replica_groups=mesh['sp'=8,'tp'=4] {'sp'}, dimensions={0}, use_global_device_ids=true | all-gather | bytes 73728 | tf_op jit(solution)/shard_map/all_gather | solution.py:35
  74.9 39.1 %all-gather.8.cloned.1.call-done = bf16[4096,256]{0,1:T(8,128)(2,1)} async-done(((bf16[512,256]{0,1:T(8,128)(2,1)}), bf16[4096,256]{0,1:T(8,128)(2,1)}) %all-gather.8.cloned.1.call-update) | async-done | bytes 2097168 | tf_op jit(solution)/shard_map/all_gather | solution.py:43
  114.1 62.3 %while.14 = (s32[]{:T(128)}, f32[512,4]{0,1:T(4,128)S(1)}, f32[512,4]{0,1:T(4,128)S(1)}, f32[512,4,64]{0,2,1:T(8,128)S(1)}, s32[8]{0:T(128)S(1)}, /*index=5*/s32...) while((s32[]{:T(128)}, f32[512,4]{0,1:T(4,128)S(1)}, ...), condition=%wide.region_5.6_spmd, body=%wide.region_0.5_spmd.sunk | while | flops 289411584 | bytes 16759253 | solution.py:89
  114.2 0.6 dynamic_slice.36
  115.5 0.6 slice.32
  116.1 1.2 slice.33
  119.1 0.6 slice.31
  120.9 7.5 %conditional.2 = (f32[512,4]{0,1:T(4,128)S(1)}, f32[512,4]{0,1:T(4,128)S(1)}, f32[512,4,64]{0,2,1:T(8,128)S(1)}) conditional(s32[]{:T(128)} %bitcast.76, (s32[512]{0:T(512)S(1)}, s32[512]{0:T(512)S(1)}, s32[512]{0:T(512)S(1)}, s32[512]{0:T(512)}, bf16[4096,256]{0,1:T(8,128)(2,1)}, /*index=5*/s32[]{:T(128)}, bf16[512,4,64]{0,2,1:T(8,128)(2,1)S(1)}, ...), branch_computations={%region_1.3_spmd, %region_4.4_spmd} | conditional | flops 289411072 | bytes 16736316 | solution.py:87
  121.0 1.3 constant_dynamic-slice_fusion
  122.4 1.0 compare_and_fusion
  123.3 1.9 fusion.4
  125.3 1.5 fusion.3
  126.8 1.6 fusion.11
  128.5 0.6 dynamic_slice.36
  130.4 1.2 slice.33
  133.4 0.6 slice.31
  135.3 0.6 dynamic_slice.36
  136.7 0.6 slice.32
  137.2 1.2 slice.33
  140.2 0.6 slice.31
  142.2 0.6 dynamic_slice.36
  143.5 0.6 slice.32
  144.1 1.2 slice.33
  147.1 0.6 slice.31
  149.0 0.6 dynamic_slice.36
  150.9 1.2 slice.33
  153.9 0.6 slice.31
  155.9 0.6 dynamic_slice.36
  157.8 1.2 slice.33
  160.8 0.6 slice.31
  162.7 0.6 dynamic_slice.36
  164.6 1.2 slice.33
  167.6 0.6 slice.31
  169.6 0.6 dynamic_slice.36
  171.5 1.2 slice.33
  174.5 0.6 slice.31
  177.2 0.7 copy.41
  177.9 3.4 all-to-all-start
  181.4 1.5 scatter_custom_fusion
  183.0 4.3 all-to-all-done
  187.3 2.9 fusion.23
  190.6 2.5 gather_fusion
  193.3 71.4 %all_to_all.26 = bf16[8,64,2048]{2,1,0:T(8,128)(2,1)} all-to-all(bf16[8,64,2048]{2,1,0:T(8,128)(2,1)S(1)} %broadcast_select_fusion), channel_id=1, replica_groups=mesh['sp'=8,'tp'=4] {'sp'}, dimensions={0} | all-to-all | bytes 4194304 | tf_op jit(solution)/shard_map/all_to_all | solution.py:123
  265.0 56.4 %all-gather.10.cloned.1.call-done = bf16[8,256,2048]{2,1,0:T(8,128)(2,1)} async-done(((bf16[8,64,2048]{2,1,0:T(8,128)(2,1)}), bf16[8,256,2048]{2,1,0:T(8,128)(2,1)}) %all-gather.10.cloned.1.call-update) | async-done | bytes 8388624 | tf_op jit(solution)/shard_map/all_gather | solution.py:122
  321.4 14.1 %fusion.20 = f32[2048,896]{1,0:T(8,128)} fusion(bf16[2048,2048]{1,0:T(8,128)(2,1)} %bitcast.90, bf16[1,2048,896]{2,1,0:T(8,128)(2,1)} %param.29), kind=kOutput, calls=%fused_computation.29 | convolution fusion | flops 7516192768 | bytes 19398656 | tf_op jit(solution)/shard_map/dot_general | solution.py:129
  335.5 25.4 %convolution_convert_fusion = bf16[2048,2048]{1,0:T(8,128)(2,1)} fusion(f32[2048,896]{1,0:T(8,128)} %fusion.20, bf16[2048,2048]{1,0:T(8,128)(2,1)} %bitcast.91, bf16[1,896,2048]{2,1,0:T(8,128)(2,1)} %param.31, bf16[1,2048,896]{2,1,0:T(8,128)(2,1)} %param.30), kind=kOutput, calls=%fused_computation.25 | convolution fusion | flops 15047589888 | bytes 31457280 | tf_op jit(solution)/shard_map/dot_general | solution.py:132
  360.9 0.6 copy-done.5
  361.5 0.6 dynamic-slice
  362.1 151.8 %all-reduce.3.cloned.1.call-done = bf16[8,4,64,2048]{3,2,1,0:T(8,128)(2,1)} async-done(((bf16[8,4,64,2048]{3,2,1,0:T(8,128)(2,1)}), bf16[8,4,64,2048]{3,2,1,0:T(8,128)(2,1)}) %all-reduce.3.cloned.1.call-update) | async-done | bytes 8388624
  513.9 3.9 dynamic-slice_bitcast_fusion.1
  517.8 5.5 all-to-all-start.2
  523.5 47.8 %all-to-all-done.2 = bf16[8,64,2048]{2,1,0:T(8,128)(2,1)S(1)} async-done(((bf16[8,64,2048]{2,1,0:T(8,128)(2,1)}), bf16[8,64,2048]{2,1,0:T(8,128)(2,1)S(1)}, u32[]{:S(2)}, u32[]{:S(2)}) %all-to-all-start.2) | async-done | bytes 2097184 | tf_op jit(solution)/shard_map/all_to_all | solution.py:138
  571.3 2.3 gather_fusion.1
  573.6 2.4 reshape.182
  576.0 3.2 multiply_reduce_fusion
  579.2 0.9 fusion.27
  (106 shorter events, 10.9 us)
Async XLA Ops:
  6.5 68.4 %all-gather.6.cloned.1.call-start = ((), (), s32[]{:S(2)}) async-start(), calls=%async_computation.3 | async-start | bytes 2359296 | tf_op jit(solution)/shard_map/all_gather | solution.py:42
  8.4 105.7 %all-gather.8.cloned.1.call-start = ((), (), s32[]{:S(2)}) async-start(), calls=%async_computation.4 | async-start | bytes 2359296 | tf_op jit(solution)/shard_map/all_gather | solution.py:43
  114.1 62.7 %copy-start.3 = (f32[256]{0:T(256)S(1)}, f32[256]{0:T(256)}, u32[]{:S(2)}) copy-start(f32[256]{0:T(256)} %param.23) | copy-start | bytes 3076
  120.9 4.4 copy-start.1
  176.4 10.9 %copy-start = (bf16[128,2048]{1,0:T(8,128)(2,1)S(1)}, bf16[128,2048]{1,0:T(8,128)(2,1)}, u32[]{:S(2)}) copy-start(bf16[128,2048]{1,0:T(8,128)(2,1)} %param.25) | copy-start | bytes 1572868
  176.8 13.6 %copy-start.2 = (f32[2048]{0:T(1024)S(1)}, f32[2048]{0:T(1024)}, u32[]{:S(2)}) copy-start(f32[2048]{0:T(1024)} %param.26) | copy-start | bytes 24580
  177.9 9.4 %all-to-all-start = ((bf16[4,128,256]{1,2,0:T(8,128)(2,1)}), bf16[4,128,256]{1,2,0:T(8,128)(2,1)S(1)}, u32[]{:S(2)}, u32[]{:S(2)}) async-start(bf16[4,128,256]{1,2,0:T(8,128)(2,1)} %copy.41), calls=%async_computation | async-start | bytes 524288 | tf_op jit(solution)/shard_map/all_to_all | solution.py:100
  181.3 140.1 %all-gather.10.cloned.1.call-start = ((), (), s32[]{:S(2)}) async-start(), calls=%async_computation.5 | async-start | bytes 10485760 | tf_op jit(solution)/shard_map/all_gather | solution.py:122
  264.8 249.2 %all-reduce.3.cloned.1.call-start = ((), (), s32[]{:S(2)}) async-start(), calls=%async_computation.6 | async-start | bytes 16777216
  360.9 0.7 copy-start.5
  513.9 9.4 %copy-start.4 = (f32[128,2]{0,1:T(2,128)S(1)}, f32[128,2]{0,1:T(2,128)}, u32[]{:S(2)}) copy-start(f32[128,2]{0,1:T(2,128)} %param.28) | copy-start | bytes 3076
  517.8 53.4 %all-to-all-start.2 = ((bf16[8,64,2048]{2,1,0:T(8,128)(2,1)}), bf16[8,64,2048]{2,1,0:T(8,128)(2,1)S(1)}, u32[]{:S(2)}, u32[]{:S(2)}) async-start(bf16[8,64,2048]{2,1,0:T(8,128)(2,1)} %dynamic-slice_bitcast_fusion.1), calls=%async_computation.2 | async-start | bytes 4194304 | tf_op jit(solution)/shard_map/all_to_all | solution.py:138
Sparse Core Ops, SparseCore 0:
  9.4 53.8 all-gather.5
  65.3 48.6 all-gather.7
  264.9 56.4 all-gather.9
  361.0 152.8 all-reduce.2
where the time goes:
time: 590 us; the launch traced here: 587 us
  waiting for transfers between devices  299 us (51%)
  blocking collectives  131 us (22%)
  local copies, waits for them, and re-layouts  52.8 us (9%)
  matrix products  46 us (8%)
  loops' own time  26 us (4%)
  between operations  13.4 us (2%)
  starting transfers between devices  9.23 us (2%)
  other arithmetic  9.14 us (2%)
    unnamed x5, waiting for transfers between devices  152 us
    all_to_all x1, blocking collectives, on_device(): lax.all_to_all(outbound, 'sp', split_axis=0, concat_axis=0, tiled=True)  71.4 us
    all_gather x1, waiting for transfers between devices, on_device(): lax.all_gather(lax.all_to_all(outbound, 'sp', split_axis=0, concat_axis=0...  56.4 us
    all_to_all x1, waiting for transfers between devices, on_device(): lax.all_to_all(summed[:, 0].astype(jnp.bfloat16), 'sp', split_axis=0, con...  47.8 us
    all_gather x1, waiting for transfers between devices, on_device(): value_part = lax.all_gather(values, 'sp', axis=0, tiled=True)  39.1 us
    all_gather x1, blocking collectives, on_device(): history = lax.all_gather(cum_gate, 'sp', axis=0, tiled=True)  31.1 us
    all_gather x1, blocking collectives, on_device(): doc_part = lax.all_gather(documents, 'sp', axis=0, tiled=True)  28.1 us
    another operation x1, loops' own time, on_device(): lax.scan(visit_block, running, jnp.arange(length // block_len, dtype=jnp....  25.7 us
  transfers between devices with their start and end apart: 6, of which 5 were waited for; matrix products, arithmetic and copies ran while one was open for 2% of the time, Pallas kernels for 0%

commit v1 on v0

v1 whole, which is shorter than its diff:
```python
import functools

import jax
import jax.numpy as jnp
from jax import lax
from jax.experimental import pallas as pl
from jax.experimental.pallas import tpu as pltpu
from jax.sharding import PartitionSpec as P

EPS = 1e-06
MESH = pl.DeviceIdType.MESH
NEG = -1e30
VMEM_LIMIT = 60 * 1024 * 1024


def attention_kernel(
    heads_here, block_len, first_ref, q_ref, kv_ref, gate_ref, start_ref, gain_ref, out_ref
):
    tokens, width_here = q_ref.shape
    head_size = width_here // heads_here
    score_scale = head_size ** (-0.5)
    first_block, own_block = first_ref[0], first_ref[1]
    blocks_own = tokens // block_len

    def visit(head, rows, offset, state, causal):
        cols = slice(head * head_size, (head + 1) * head_size)
        vcols = slice(width_here + head * head_size, width_here + (head + 1) * head_size)
        row_max, row_sum, weighted = state
        offset = pl.multiple_of(offset, block_len)
        k = kv_ref[pl.ds(offset, block_len), cols]
        v = kv_ref[pl.ds(offset, block_len), vcols]
        gate = gate_ref[head : head + 1, pl.ds(offset, block_len)]
        base = gate_ref[head : head + 1, pl.ds(pl.multiple_of(own_block * tokens, tokens), 128)][
            :, :1
        ]
        scores = (
            lax.dot_general(
                q_ref[rows, cols],
                k,
                (((1,), (1,)), ((), ())),
                preferred_element_type=jnp.float32,
            )
            * score_scale
        )
        scores = scores + (base - gate)
        key_pos = offset + lax.broadcasted_iota(jnp.int32, (1, block_len), 1)
        allowed = key_pos >= start_ref[rows, :]
        if causal:
            query_pos = (
                own_block * tokens
                + rows.start
                + lax.broadcasted_iota(jnp.int32, (block_len, 1), 0)
            )
            allowed = allowed & (key_pos <= query_pos)
        scores = jnp.where(allowed, scores, NEG)
        next_max = jnp.maximum(row_max, jnp.max(scores, axis=-1, keepdims=True))
        exps = jnp.exp(scores - next_max)
        rescale = jnp.exp(row_max - next_max)
        row_sum = row_sum * rescale + jnp.sum(exps, axis=-1, keepdims=True)
        weighted = weighted * rescale + jnp.dot(
            exps.astype(jnp.bfloat16), v, preferred_element_type=jnp.float32
        )
        return next_max, row_sum, weighted

    for part in range(blocks_own):
        rows = slice(part * block_len, (part + 1) * block_len)
        outs = []
        for head in range(heads_here):
            state = (
                jnp.full((block_len, 1), NEG, jnp.float32),
                jnp.zeros((block_len, 1), jnp.float32),
                jnp.zeros((block_len, head_size), jnp.float32),
            )
            diagonal = own_block * blocks_own + part
            state = visit(head, rows, diagonal * block_len, state, True)
            state = lax.fori_loop(
                first_block,
                diagonal,
                lambda j, s: visit(head, rows, j * block_len, s, False),
                state,
            )
            attended = state[2] / state[1]
            mean_square = jnp.mean(attended * attended, axis=-1, keepdims=True)
            outs.append(attended * lax.rsqrt(mean_square + EPS))
        normed = jnp.concatenate(outs, axis=-1) * gain_ref[...]
        out_ref[rows, :] = normed.astype(jnp.bfloat16)


def expert_kernel(
    n,
    out_ref,
    wg_hbm,
    wu_hbm,
    wd_hbm,
    ret_ref,
    fan,
    wg,
    wu,
    wd,
    hidden,
    part,
    got,
    pair,
    across,
    fin,
    w_sem,
    own_sem,
    a_send,
    a_recv,
    x_send,
    x_recv,
    c_send,
    c_recv,
    d_send,
    d_recv,
    p_send,
    p_recv,
    s_send,
    s_recv,
    r_send,
    r_recv,
):
    me = lax.axis_index("sp")
    t = lax.axis_index("tp")
    c, xi = lax.rem(t, 2), t // 2
    near = xi * 2 + (1 - c)
    far = (1 - xi) * 2 + c
    cap, width = out_ref.shape[1], out_ref.shape[2]
    near_id = {"sp": me, "tp": near}
    far_id = {"sp": me, "tp": far}

    weights = [
        pltpu.make_async_copy(src, dst, w_sem.at[i])
        for i, (src, dst) in enumerate(((wg_hbm, wg), (wu_hbm, wu), (wd_hbm, wd)))
    ]
    for copy in weights:
        copy.start()

    barrier = pltpu.get_barrier_semaphore()

    def greet(k, carry):
        pl.semaphore_signal(
            barrier,
            inc=1,
            device_id={"sp": lax.rem(me + k, n), "tp": t},
            device_id_type=MESH,
        )
        return carry

    lax.fori_loop(1, n, greet, 0)
    for other in (near_id, far_id):
        pl.semaphore_signal(barrier, inc=1, device_id=other, device_id_type=MESH)
    pl.semaphore_wait(barrier, n + 1)

    def remote(src, dst, send, recv, to):
        return pltpu.make_async_remote_copy(
            src_ref=src, dst_ref=dst, send_sem=send, recv_sem=recv, device_id=to, device_id_type=MESH
        )

    def source(k):
        return lax.rem(me - k + n, n)

    def a_out(k):
        to = lax.rem(me + k, n)
        return remote(
            out_ref.at[to], fan.at[me, t], a_send.at[k], a_recv.at[me], {"sp": to, "tp": t}
        )

    def a_in(k):
        p = source(k)
        return remote(out_ref.at[p], fan.at[p, t], a_send.at[k], a_recv.at[p], near_id)

    def x_copy(k, q):
        p = source(k)
        return remote(fan.at[p, q], fan.at[p, q], x_send.at[p], x_recv.at[p], far_id)

    def c_copy(k, q):
        p = source(k)
        return remote(fan.at[p, q], fan.at[p, q], c_send.at[p], c_recv.at[p], near_id)

    def d_copy(k, q):
        p = source(k)
        return remote(fan.at[p, q], fan.at[p, q], d_send.at[p], d_recv.at[p], near_id)

    def p_copy(k):
        p = source(k)
        return remote(part.at[p, 1 - c], got.at[p], p_send.at[p], p_recv.at[p], near_id)

    def s_copy(k):
        p = source(k)
        return remote(pair.at[p], across.at[p], s_send.at[p], s_recv.at[p], far_id)

    def r_out(k):
        p = source(k)
        return remote(fin.at[p], ret_ref.at[me], r_send.at[p], r_recv.at[me], {"sp": p, "tp": t})

    def r_in(k):
        p = source(k)
        return remote(fin.at[p], ret_ref.at[p], r_send.at[p], r_recv.at[p], near_id)

    own = pltpu.make_async_copy(out_ref.at[me], fan.at[me, t], own_sem)
    own.start()
    lax.fori_loop(1, n, lambda k, z: (a_out(k).start(), z)[1], 0)

    def forward(k):
        x_copy(k, t).start()
        c_copy(k, t).start()

    own.wait()
    forward(0)

    def step_a(k):
        a_in(k).wait_recv()
        forward(k)

    def step_x(k):
        x_copy(k, far).wait_recv()
        d_copy(k, far).start()

    def step_compute(k):
        p = source(k)
        c_copy(k, near).wait_recv()
        d_copy(k, 3 - t).wait_recv()
        rows = fan[p].reshape(4 * cap, width)
        gate = jnp.dot(rows, wg[...], preferred_element_type=jnp.float32)
        up = jnp.dot(rows, wu[...], preferred_element_type=jnp.float32)
        hidden[...] = (gate * jax.nn.sigmoid(gate) * up).astype(jnp.bfloat16)
        tile = 512 if width % 512 == 0 else width
        for at in range(0, width, tile):
            down = jnp.dot(
                hidden[...], wd[:, at : at + tile], preferred_element_type=jnp.float32
            ).astype(jnp.bfloat16)
            for q in range(4):
                part[p, q % 2, q // 2, :, at : at + tile] = down[q * cap : (q + 1) * cap]
        p_copy(k).start()

    def step_pair(k):
        p = source(k)
        p_copy(k).wait_recv()
        pair[p] = (
            part[p, c, 1 - xi].astype(jnp.float32) + got[p, 1 - xi].astype(jnp.float32)
        ).astype(jnp.bfloat16)
        s_copy(k).start()

    def step_final(k):
        p = source(k)
        s_copy(k).wait_recv()
        total = (
            part[p, c, xi].astype(jnp.float32)
            + got[p, xi].astype(jnp.float32)
            + across[p].astype(jnp.float32)
        ).astype(jnp.bfloat16)

        @pl.when(k == 0)
        def _():
            ret_ref[me] = total

        @pl.when(k > 0)
        def _():
            fin[p] = total
            r_out(k).start()

    step_a(1)
    step_x(0)
    for copy in weights:
        copy.wait()

    def iteration(i, carry):
        @pl.when(i + 2 < n)
        def _():
            step_a(i + 2)

        @pl.when(i + 1 < n)
        def _():
            step_x(i + 1)

        @pl.when((i >= 1) & (i < n + 1))
        def _():
            step_pair(i - 1)

        @pl.when(i < n)
        def _():
            step_compute(i)

        @pl.when(i >= 2)
        def _():
            step_final(i - 2)

        return carry

    lax.fori_loop(0, n + 2, iteration, 0)

    def finish(k, carry):
        x_copy(k, t).wait_send()
        c_copy(k, t).wait_send()
        d_copy(k, far).wait_send()
        p_copy(k).wait_send()
        s_copy(k).wait_send()

        @pl.when(k > 0)
        def _():
            a_out(k).wait_send()
            r_out(k).wait_send()
            r_in(k).wait_recv()

        return carry

    lax.fori_loop(0, n, finish, 0)


def experts(n, outbound, w_gate, w_up, w_down):
    _, cap, width = outbound.shape
    hid = w_gate.shape[1]
    bf = jnp.bfloat16
    dma = pltpu.SemaphoreType.DMA
    hbm = pl.BlockSpec(memory_space=pl.ANY)
    vmem = pl.BlockSpec(memory_space=pltpu.VMEM)
    return pl.pallas_call(
        functools.partial(expert_kernel, n),
        out_shape=jax.ShapeDtypeStruct((n, cap, width), bf),
        in_specs=[vmem, hbm, hbm, hbm],
        out_specs=vmem,
        scratch_shapes=[
            pltpu.VMEM((n, 4, cap, width), bf),
            pltpu.VMEM((width, hid), bf),
            pltpu.VMEM((width, hid), bf),
            pltpu.VMEM((hid, width), bf),
            pltpu.VMEM((4 * cap, hid), bf),
            pltpu.VMEM((n, 2, 2, cap, width), bf),
            pltpu.VMEM((n, 2, cap, width), bf),
            pltpu.VMEM((n, cap, width), bf),
            pltpu.VMEM((n, cap, width), bf),
            pltpu.VMEM((n, cap, width), bf),
            dma((3,)),
            dma,
        ]
        + [dma((n,)) for _ in range(14)],
        compiler_params=pltpu.CompilerParams(
            collective_id=1, has_side_effects=True, vmem_limit_bytes=VMEM_LIMIT
        ),
    )(outbound, w_gate, w_up, w_down)


def on_device(
    queries,
    keys,
    values,
    cum_gate,
    documents,
    head_gain,
    out_weight,
    resid,
    norm_gain,
    routes,
    route_weights,
    w_gate,
    w_up,
    w_down,
):
    bf = jnp.bfloat16
    tokens = queries.shape[0]
    heads_here = cum_gate.shape[1]
    width_here = queries.shape[1]
    me = lax.axis_index("sp")
    high = lax.reduce_precision(cum_gate, 8, 7)
    middle = lax.reduce_precision(cum_gate - high, 8, 7)
    low = cum_gate - high - middle
    extra = jnp.concatenate(
        [high, middle, low, documents[:, None].astype(jnp.float32)], axis=1
    ).astype(bf)
    pad = -extra.shape[1] % 128
    packed = jnp.concatenate([keys, values, jnp.pad(extra, ((0, 0), (0, pad)))], axis=1)
    packed = lax.all_gather(packed, "sp", axis=0, tiled=True)
    tail = packed[:, 2 * width_here :].astype(jnp.float32)
    gates = (
        tail[:, :heads_here]
        + tail[:, heads_here : 2 * heads_here]
        + tail[:, 2 * heads_here : 3 * heads_here]
    ).T
    all_docs = tail[:, 3 * heads_here].astype(jnp.int32)
    starts = jnp.sum(
        (all_docs[None, :] < documents[:, None]).astype(jnp.int32), axis=1, keepdims=True
    )
    block_len = min(tokens, 512)
    first = jnp.stack([starts[0, 0] // block_len, me]).astype(jnp.int32)
    vmem = pl.BlockSpec(memory_space=pltpu.VMEM)
    head_normed = pl.pallas_call(
        functools.partial(attention_kernel, heads_here, block_len),
        out_shape=jax.ShapeDtypeStruct((tokens, width_here), bf),
        in_specs=[pl.BlockSpec(memory_space=pltpu.SMEM)] + [vmem] * 5,
        out_specs=vmem,
        compiler_params=pltpu.CompilerParams(vmem_limit_bytes=VMEM_LIMIT),
    )(first, queries, packed, gates, starts, head_gain[None, :])

    regrouped = lax.all_to_all(head_normed, "tp", split_axis=0, concat_axis=1, tiled=True)
    projected = jnp.dot(regrouped, out_weight, preferred_element_type=jnp.float32)
    stream = lax.optimization_barrier((resid.astype(jnp.float32) + projected).astype(bf))
    widened = stream.astype(jnp.float32)
    mean_wide = jnp.mean(widened * widened, axis=-1, keepdims=True)
    expert_input = (widened * lax.rsqrt(mean_wide + EPS) * norm_gain).astype(bf)

    local_rows, top_count = routes.shape
    expert_count = lax.axis_size("sp")
    tp_count = lax.axis_size("tp")
    capacity = 2 * top_count * tokens // (tp_count * expert_count)
    flat_routes = routes.reshape(-1)
    onehot = (flat_routes[:, None] == jnp.arange(expert_count, dtype=jnp.int32)[None, :]).astype(
        jnp.float32
    )
    order = jnp.arange(flat_routes.shape[0], dtype=jnp.int32)
    earlier = (order[None, :] < order[:, None]).astype(bf)
    counts = jnp.dot(earlier, onehot.astype(bf), preferred_element_type=jnp.float32)
    ranks = jnp.sum(counts * onehot, axis=1).astype(jnp.int32)
    targets = (flat_routes * capacity + ranks).reshape(local_rows, top_count)
    slots = jnp.arange(expert_count * capacity, dtype=jnp.int32)
    picks = targets[:, :, None] == slots[None, None, :]
    into = jnp.any(picks, axis=1).astype(bf)
    outbound = lax.dot_general(
        into, expert_input, (((0,), (0,)), ((), ())), preferred_element_type=jnp.float32
    ).astype(bf)
    outbound = outbound.reshape(expert_count, capacity, -1)
    returned = experts(expert_count, outbound, w_gate[0], w_up[0], w_down[0])
    returned = returned.reshape(expert_count * capacity, -1)
    mixed = widened
    for route in range(top_count):
        chosen = jnp.dot(
            picks[:, route].astype(bf), returned, preferred_element_type=jnp.float32
        )
        mixed = mixed + route_weights[:, route : route + 1] * chosen
    return mixed.astype(bf)


def solution(mesh):
    in_specs = (
        P("sp", "tp"),
        P("sp", "tp"),
        P("sp", "tp"),
        P("sp", "tp"),
        P("sp"),
        P("tp"),
        P(),
        P(("sp", "tp"), None),
        P(),
        P(("sp", "tp"), None),
        P(("sp", "tp"), None),
        P("sp", None, "tp"),
        P("sp", None, "tp"),
        P("sp", "tp", None),
    )
    out_specs = P(("sp", "tp"), None)
    return jax.shard_map(
        on_device, mesh=mesh, in_specs=in_specs, out_specs=out_specs, check_vma=False
    )
```

time: 590 us -> 294 us (0.50)
  waiting for transfers between devices: 299 us -> 94.5 us
  Pallas kernels: 0 us -> 150 us
  blocking collectives: 131 us -> 0 us
  local copies, waits for them, and re-layouts: 52.8 us -> 13.7 us
  matrix products: 46 us -> 8.77 us
  loops' own time: 26 us -> 0 us
    unnamed x5 -> x1, waiting for transfers between devices: 152 us -> 0.02 us
    pallas_call x0 -> x2, Pallas kernels: none -> 150 us  [the longest x1 143 us: experts(): pl.pallas_call(functools.partial(expert_kernel, n), out_shape=jax.ShapeDt...]
    all_to_all x1 -> x0, blocking collectives: 71.4 us -> none  [on_device(): lax.all_to_all(outbound, 'sp', split_axis=0, concat_axis=0, tiled=True)]
    all_gather x2 -> x0, blocking collectives: 59.2 us -> none  [the longest x1 31.1 us: on_device(): history = lax.all_gather(cum_gate, 'sp', axis=0, tiled=True)]
    all_to_all x1 -> x0, waiting for transfers between devices: 47.8 us -> none  [on_device(): lax.all_to_all(summed[:, 0].astype(jnp.bfloat16), 'sp', split_axis=0, con...]
    dot_general x4, matrix products: 43 us -> 5.83 us  [the longest x2 3.49 us: on_device(): jnp.dot(picks[:, route].astype(bf), returned, preferred_element_type=jnp....]
    another operation x9 -> x0, loops' own time: 26 us -> none  [the longest x1 25.7 us: on_device(): lax.scan(visit_block, running, jnp.arange(length // block_len, dtype=jnp....]
    slice x33 -> x1, local copies, waits for them, and re-layouts: 23.6 us -> 0.52 us  [on_device(): first = jnp.stack([starts[0, 0] // block_len, me]).astype(jnp.int32)]
  transfers between devices with their start and end apart: 6 -> 2, of which waited for: 5 -> 2; matrix products, arithmetic and copies ran while one was open for 2% -> 0% of each run, Pallas kernels for 0% -> 0%
where the time goes in v1:
time: 294 us; the launch traced here: 293 us
  Pallas kernels  150 us (51%)
  waiting for transfers between devices  94.5 us (32%)
  between operations  16.2 us (6%)
  local copies, waits for them, and re-layouts  13.7 us (5%)
  matrix products  8.77 us (3%)
  other arithmetic  6.42 us (2%)
  starting transfers between devices  3.59 us (1%)
    pallas_call x1, Pallas kernels, experts(): pl.pallas_call(functools.partial(expert_kernel, n), out_shape=jax.ShapeDt...  143 us
    all_gather x1, waiting for transfers between devices, on_device(): packed = lax.all_gather(packed, 'sp', axis=0, tiled=True)  88.8 us
    all_gather x1, local copies, waits for them, and re-layouts, on_device(): packed = lax.all_gather(packed, 'sp', axis=0, tiled=True)  7.85 us
    pallas_call x1, Pallas kernels, on_device(): pl.pallas_call(functools.partial(attention_kernel, heads_here, block_len)...  6.87 us
  transfers between devices with their start and end apart: 2, of which 2 were waited for; matrix products, arithmetic and copies ran while one was open for 0% of the time, Pallas kernels for 0%

profile of v1, /device:TPU:0, one launch (start us, length us, event | category | flops | bytes accessed | tf_op | source)
XLA Modules:
  0.0 293.2 jit_solution(2800032004085745914)
XLA Ops:
  6.5 0.0 copy-start.3
  6.5 0.0 all-gather.2.cloned.1.call-start
  6.5 0.7 reduce-precision_convert_fusion.1
  7.3 0.7 convert_convert_fusion.2
  7.9 1.1 copy.37
  9.0 1.1 copy.38
  10.2 0.9 pad_maximum_fusion
  11.1 0.0 copy-start.4
  11.1 0.0 all-gather.2.cloned.1.call-update
  11.1 0.0 copy-done.3
  11.1 0.1 copy.42
  11.2 0.1 eq.28
  11.4 0.2 fusion.4
  11.6 0.1 convert_element_type.73
  11.7 0.1 copy.43
  11.8 0.2 iota_compare_fusion
  12.0 88.8 %all-gather.2.cloned.1.call-done = bf16[4096,640]{0,1:T(8,128)(2,1)} async-done(((bf16[512,640]{0,1:T(8,128)(2,1)}), bf16[4096,640]{0,1:T(8,128)(2,1)}) %all-gather.2.cloned.1.call-update) | async-done | bytes 5242896 | tf_op jit(solution)/shard_map/all_gather | solution.py:373
  100.8 1.4 slice_convert_fusion
  102.2 0.0 copy-done.4
  102.2 1.0 convert_reduce_fusion
  103.2 0.5 slice.33
  105.1 0.7 fusion.18.gate_ref
  107.0 0.9 copy.40.start_ref
  107.9 0.6 pad_add_fusion.first_ref
  108.5 7.9 %copy.39.kv_ref = bf16[4096,640]{1,0:T(8,128)(2,1)} copy(bf16[4096,640]{0,1:T(8,128)(2,1)} %all-gather.2.cloned.1.call-done) | data formatting | bytes 10485760 | tf_op jit(solution)/shard_map/all_gather | solution.py:373
  116.3 0.0 copy-start.5
  116.3 0.0 copy-start.1
  116.3 6.9 %shard_map.136 = bf16[512,256]{1,0:T(8,128)(2,1)} custom-call(s32[2]{0:T(128)} %pad_add_fusion.first_ref, bf16[512,256]{1,0:T(8,128)(2,1)} %q_ref.1, bf16[4096,640]{1,0:T(8,128)(2,1)} %copy.39.kv_ref, f32[4,4096]{1,0:T(4,128)} %fusion.18.gate_ref, s32[512,1]{1,0:T(8,128)} %copy.40.start_ref, f32[1,256]{1,0:T(1,128)} %bitcast.42), custom_call_target="tpu_custom_call" | custom-call | tf_op jit(solution)/shard_map/pallas_call | solution.py:387
  123.2 1.8 copy.41
  125.0 3.6 %all-to-all-start = ((bf16[4,128,256]{1,2,0:T(8,128)(2,1)}), bf16[4,128,256]{1,2,0:T(8,128)(2,1)S(1)}, u32[]{:S(2)}, u32[]{:S(2)}) async-start(bf16[4,128,256]{1,2,0:T(8,128)(2,1)} %copy.41), calls=%async_computation | async-start | bytes 524288 | tf_op jit(solution)/shard_map/all_to_all | solution.py:395
  128.6 0.0 copy-done.5
  128.6 5.8 %all-to-all-done = bf16[4,128,256]{1,2,0:T(8,128)(2,1)S(1)} async-done(((bf16[4,128,256]{1,2,0:T(8,128)(2,1)}), bf16[4,128,256]{1,2,0:T(8,128)(2,1)S(1)}, u32[]{:S(2)}, u32[]{:S(2)}) %all-to-all-start) | async-done | bytes 262176 | tf_op jit(solution)/shard_map/all_to_all | solution.py:395
  134.4 0.0 copy-done.1
  134.4 0.0 copy-start.2
  134.4 2.9 %fusion.2 = bf16[128,2048]{1,0:T(8,128)(2,1)S(1)} fusion(bf16[128,1024]{0,1:T(8,128)(2,1)S(1)} %bitcast.38, bf16[1024,2048]{1,0:T(8,128)(2,1)} %param.20, bf16[128,2048]{1,0:T(8,128)(2,1)S(1)} %copy-done.1), kind=kOutput, calls=%fused_computation.7 | convolution fusion | flops 537657344 | bytes 5505024 | tf_op jit(solution)/shard_map/dot_general | solution.py:396
  137.3 0.2 fusion.5
  137.5 0.0 copy-done.2
  137.5 2.1 convolution_convert_fusion
  139.7 143.1 %shard_map.137 = bf16[8,64,2048]{2,1,0:T(8,128)(2,1)} custom-call(bf16[8,64,2048]{2,1,0:T(8,128)(2,1)} %bitcast.34, bf16[2048,896]{1,0:T(8,128)(2,1)} %bitcast.35, bf16[2048,896]{1,0:T(8,128)(2,1)} %bitcast.36, bf16[896,2048]{1,0:T(8,128)(2,1)} %bitcast.37), custom_call_target="tpu_custom_call" | custom-call | tf_op jit(solution)/shard_map/pallas_call | solution.py:318
  282.8 0.0 copy-start
  282.8 2.2 fusion.1
  285.0 0.0 copy-done
  285.0 1.3 fusion.3
  (7 shorter events, 0.1 us)
Async XLA Ops:
  6.5 4.6 %copy-start.3 = (s32[128,2]{0,1:T(2,128)S(1)}, s32[128,2]{0,1:T(2,128)}, u32[]{:S(2)}) copy-start(s32[128,2]{0,1:T(2,128)} %param.23) | copy-start | bytes 3076
  6.5 94.2 %all-gather.2.cloned.1.call-start = ((), (), s32[]{:S(2)}) async-start(), calls=%async_computation.1 | async-start | bytes 5898240 | tf_op jit(solution)/shard_map/all_gather | solution.py:373
  11.1 91.1 %copy-start.4 = (s32[512]{0:T(512)S(1)}, s32[512]{0:T(512)}, u32[]{:S(2)}) copy-start(s32[512]{0:T(512)} %param.18) | copy-start | bytes 6148
  116.3 12.3 %copy-start.5 = (f32[128,2]{0,1:T(2,128)S(1)}, f32[128,2]{0,1:T(2,128)}, u32[]{:S(2)}) copy-start(f32[128,2]{0,1:T(2,128)} %param.24) | copy-start | bytes 3076
  116.3 18.0 %copy-start.1 = (bf16[128,2048]{1,0:T(8,128)(2,1)S(1)}, bf16[128,2048]{1,0:T(8,128)(2,1)}, u32[]{:S(2)}) copy-start(bf16[128,2048]{1,0:T(8,128)(2,1)} %param.21) | copy-start | bytes 1572868
  125.0 9.4 %all-to-all-start = ((bf16[4,128,256]{1,2,0:T(8,128)(2,1)}), bf16[4,128,256]{1,2,0:T(8,128)(2,1)S(1)}, u32[]{:S(2)}, u32[]{:S(2)}) async-start(bf16[4,128,256]{1,2,0:T(8,128)(2,1)} %copy.41), calls=%async_computation | async-start | bytes 524288 | tf_op jit(solution)/shard_map/all_to_all | solution.py:395
  134.4 3.1 %copy-start.2 = (f32[2048]{0:T(1024)S(1)}, f32[2048]{0:T(1024)}, u32[]{:S(2)}) copy-start(f32[2048]{0:T(1024)} %param.22) | copy-start | bytes 24580
  282.8 2.2 copy-start
Sparse Core Ops, SparseCore 0:
  11.2 89.4 all-gather.1

commit v2 on v1

--- a/solution.py
+++ b/solution.py
@@ -341,6 +341,109 @@
     )(outbound, w_gate, w_up, w_down)
 
 
+def history_kernel(n, own_ref, all_ref, own_sem, up_send, up_recv, mate_send, mate_recv):
+    me = lax.axis_index("sp")
+    y, z = lax.rem(me, 2), me // 2
+    floors, reach = n // 2, n // 4
+    mate_id = {"sp": me + 1 - 2 * y}
+    above_id = {"sp": lax.rem(me + 2, n)}
+    below_id = {"sp": lax.rem(me + n - 2, n)}
+    barrier = pltpu.get_barrier_semaphore()
+    for other in (mate_id, above_id, below_id):
+        pl.semaphore_signal(barrier, inc=1, device_id=other, device_id_type=MESH)
+    pl.semaphore_wait(barrier, 3)
+
+    def remote(src, block, send, recv, to):
+        return pltpu.make_async_remote_copy(
+            src_ref=src,
+            dst_ref=all_ref.at[block],
+            send_sem=send,
+            recv_sem=recv,
+            device_id=to,
+            device_id_type=MESH,
+        )
+
+    def up(d, src, block):
+        return remote(src, block, up_send.at[d], up_recv.at[d], above_id)
+
+    def over(d, src, block):
+        return remote(src, block, mate_send.at[d], mate_recv.at[d], mate_id)
+
+    own = pltpu.make_async_copy(own_ref, all_ref.at[me], own_sem)
+    own.start()
+
+    def sends(d):
+        rising = (z + 1 < floors) & (z >= d) if d < reach else None
+        if d == 0:
+            crossing = y == 0
+        elif d == reach:
+            crossing = (y == 1) & (z >= d)
+        else:
+            crossing = z >= d
+        return rising, crossing
+
+    def block_of(d):
+        return jnp.maximum(me - 2 * d, 0)
+
+    for d in range(reach + 1):
+        src = own_ref if d == 0 else all_ref.at[block_of(d)]
+        if d > 0:
+            @pl.when(z >= d)
+            def _():
+                up(d - 1, src, block_of(d)).wait_recv()
+
+        rising, crossing = sends(d)
+        if rising is not None:
+            @pl.when(rising)
+            def _():
+                up(d, src, block_of(d)).start()
+
+        @pl.when(crossing)
+        def _():
+            over(d, src, block_of(d)).start()
+
+    for d in range(reach + 1):
+        src = own_ref if d == 0 else all_ref.at[block_of(d)]
+        theirs = jnp.maximum(me + 1 - 2 * y - 2 * d, 0)
+        if d == 0:
+            coming = y == 1
+        elif d == reach:
+            coming = (y == 0) & (z >= d)
+        else:
+            coming = z >= d
+
+        @pl.when(coming)
+        def _():
+            over(d, own_ref, theirs).wait_recv()
+
+        rising, crossing = sends(d)
+        if rising is not None:
+            @pl.when(rising)
+            def _():
+                up(d, src, block_of(d)).wait_send()
+
+        @pl.when(crossing)
+        def _():
+            over(d, src, block_of(d)).wait_send()
+
+    own.wait()
+
+
+def gather_history(n, packed):
+    tokens, wide = packed.shape
+    steps = n // 4 + 1
+    dma = pltpu.SemaphoreType.DMA
+    gathered = pl.pallas_call(
+        functools.partial(history_kernel, n),
+        out_shape=jax.ShapeDtypeStruct((n, tokens, wide), packed.dtype),
+        in_specs=[pl.BlockSpec(memory_space=pltpu.VMEM)],
+        out_specs=pl.BlockSpec(memory_space=pl.ANY),
+        scratch_shapes=[dma] + [dma((steps,)) for _ in range(4)],
+        compiler_params=pltpu.CompilerParams(collective_id=2, has_side_effects=True),
+    )(packed)
+    return gathered.reshape(n * tokens, wide)
+
+
 def on_device(
     queries,
     keys,
@@ -370,7 +473,8 @@
     ).astype(bf)
     pad = -extra.shape[1] % 128
     packed = jnp.concatenate([keys, values, jnp.pad(extra, ((0, 0), (0, pad)))], axis=1)
-    packed = lax.all_gather(packed, "sp", axis=0, tiled=True)
+    n = lax.axis_size("sp")
+    packed = gather_history(n, packed)
     tail = packed[:, 2 * width_here :].astype(jnp.float32)
     gates = (
         tail[:, :heads_here]
@@ -378,9 +482,11 @@
         + tail[:, 2 * heads_here : 3 * heads_here]
     ).T
     all_docs = tail[:, 3 * heads_here].astype(jnp.int32)
-    starts = jnp.sum(
-        (all_docs[None, :] < documents[:, None]).astype(jnp.int32), axis=1, keepdims=True
-    )
+    oldest = jnp.maximum(me - n // 2, 0) * tokens
+    position = jnp.arange(n * tokens, dtype=jnp.int32)
+    held = (position >= oldest) & (position < (me + 1) * tokens)
+    before = (all_docs[None, :] < documents[:, None]) & held[None, :]
+    starts = oldest + jnp.sum(before.astype(jnp.int32), axis=1, keepdims=True)
     block_len = min(tokens, 512)
     first = jnp.stack([starts[0, 0] // block_len, me]).astype(jnp.int32)
     vmem = pl.BlockSpec(memory_space=pltpu.VMEM)

time: 294 us -> 230 us (0.78)
  waiting for transfers between devices: 94.5 us -> 4.88 us
  Pallas kernels: 150 us -> 197 us
  between operations: 16.2 us -> 2.8 us
  local copies, waits for them, and re-layouts: 13.7 us -> 6.03 us
    all_gather x1 -> x0, waiting for transfers between devices: 88.8 us -> none  [on_device(): packed = lax.all_gather(packed, 'sp', axis=0, tiled=True)]
    pallas_call x1, Pallas kernels: 143 us -> 170 us  [experts(): pl.pallas_call(functools.partial(expert_kernel, n), out_shape=jax.ShapeDt...]
    pallas_call x0 -> x1, Pallas kernels: none -> 20.3 us  [gather_history(): pl.pallas_call(functools.partial(history_kernel, n), out_shape=jax.ShapeD...]
    all_gather x1 -> x0, local copies, waits for them, and re-layouts: 7.85 us -> none  [on_device(): packed = lax.all_gather(packed, 'sp', axis=0, tiled=True)]
  transfers between devices with their start and end apart: 2 -> 1, of which waited for: 2 -> 1; matrix products, arithmetic and copies ran while one was open for 0% -> 0% of each run, Pallas kernels for 0% -> 0%
where the time goes in v2:
time: 230 us
  Pallas kernels  197 us (86%)
  matrix products  8.79 us (4%)
  other arithmetic  6.66 us (3%)
  local copies, waits for them, and re-layouts  6.03 us (3%)
  waiting for transfers between devices  4.88 us (2%)
  starting transfers between devices  3.59 us (2%)
  between operations  2.8 us (1%)
    pallas_call x1, Pallas kernels, experts(): pl.pallas_call(functools.partial(expert_kernel, n), out_shape=jax.ShapeDt...  170 us
    pallas_call x1, Pallas kernels, gather_history(): pl.pallas_call(functools.partial(history_kernel, n), out_shape=jax.ShapeD...  20.3 us
    pallas_call x1, Pallas kernels, on_device(): pl.pallas_call(functools.partial(attention_kernel, heads_here, block_len)...  6.89 us
    all_to_all x1, waiting for transfers between devices, on_device(): lax.all_to_all(head_normed, 'tp', split_axis=0, concat_axis=1, tiled=True)  4.88 us
  transfers between devices with their start and end apart: 1, of which 1 were waited for; matrix products, arithmetic and copies ran while one was open for 0% of the time, Pallas kernels for 0%

profile of v2, /device:TPU:0, one launch (start us, length us, event | category | flops | bytes accessed | tf_op | source)
XLA Modules:
  0.0 229.8 jit_solution(260918134940012496)
XLA Ops:
  0.0 0.7 reduce-precision_convert_fusion.1
  0.7 0.7 convert_convert_fusion.2
  1.4 0.2 copy.49
  1.6 1.9 fusion.9.own_ref
  3.5 20.3 %shard_map.136 = bf16[8,512,640]{2,1,0:T(8,128)(2,1)} custom-call(bf16[512,640]{1,0:T(8,128)(2,1)} %fusion.9.own_ref), custom_call_target="tpu_custom_call" | custom-call | tf_op jit(solution)/shard_map/pallas_call | solution.py:436
  23.8 1.3 slice.41
  25.1 0.5 copy.57
  25.6 0.0 copy-start.4
  25.6 0.2 convert_element_type.64
  25.9 0.4 copy-done.4
  26.3 1.4 convert_reduce_fusion
  27.7 0.5 slice.33
  30.1 0.7 fusion.13.gate_ref
  31.5 0.9 copy.52.start_ref
  32.3 0.7 pad_add_fusion.first_ref
  33.0 0.0 copy-start.3
  33.0 0.0 copy-start.5
  33.0 0.0 copy-start.1
  33.0 6.9 %shard_map.137 = bf16[512,256]{1,0:T(8,128)(2,1)} custom-call(s32[2]{0:T(128)} %pad_add_fusion.first_ref, bf16[512,256]{1,0:T(8,128)(2,1)} %q_ref.1, bf16[4096,640]{1,0:T(8,128)(2,1)} %bitcast.34, f32[4,4096]{1,0:T(4,128)} %fusion.13.gate_ref, s32[512,1]{1,0:T(8,128)} %copy.52.start_ref, f32[1,256]{1,0:T(1,128)} %bitcast.45), custom_call_target="tpu_custom_call" | custom-call | tf_op jit(solution)/shard_map/pallas_call | solution.py:493
  39.9 1.8 copy.53
  41.7 3.6 %all-to-all-start = ((bf16[4,128,256]{1,2,0:T(8,128)(2,1)}), bf16[4,128,256]{1,2,0:T(8,128)(2,1)S(1)}, u32[]{:S(2)}, u32[]{:S(2)}) async-start(bf16[4,128,256]{1,2,0:T(8,128)(2,1)} %copy.53), calls=%async_computation | async-start | bytes 524288 | tf_op jit(solution)/shard_map/all_to_all | solution.py:501
  45.3 0.0 copy-done.3
  45.3 0.1 copy.54
  45.4 0.1 eq.28
  45.5 0.2 fusion.5
  45.8 0.1 convert_element_type.73
  45.9 0.1 copy.55
  46.0 0.2 iota_compare_fusion.1
  46.2 0.0 copy-done.5
  46.2 4.9 %all-to-all-done = bf16[4,128,256]{1,2,0:T(8,128)(2,1)S(1)} async-done(((bf16[4,128,256]{1,2,0:T(8,128)(2,1)}), bf16[4,128,256]{1,2,0:T(8,128)(2,1)S(1)}, u32[]{:S(2)}, u32[]{:S(2)}) %all-to-all-start) | async-done | bytes 262176 | tf_op jit(solution)/shard_map/all_to_all | solution.py:501
  51.1 0.0 copy-done.1
  51.1 0.0 copy-start.2
  51.1 2.9 %fusion.2 = bf16[128,2048]{1,0:T(8,128)(2,1)S(1)} fusion(bf16[128,1024]{0,1:T(8,128)(2,1)S(1)} %bitcast.41, bf16[1024,2048]{1,0:T(8,128)(2,1)} %param.20, bf16[128,2048]{1,0:T(8,128)(2,1)S(1)} %copy-done.1), kind=kOutput, calls=%fused_computation.7 | convolution fusion | flops 537657344 | bytes 5505024 | tf_op jit(solution)/shard_map/dot_general | solution.py:502
  54.0 0.2 fusion.6
  54.2 0.0 copy-done.2
  54.2 2.2 convolution_convert_fusion
  56.4 169.9 %shard_map.138 = bf16[8,64,2048]{2,1,0:T(8,128)(2,1)} custom-call(bf16[8,64,2048]{2,1,0:T(8,128)(2,1)} %bitcast.37, bf16[2048,896]{1,0:T(8,128)(2,1)} %bitcast.38, bf16[2048,896]{1,0:T(8,128)(2,1)} %bitcast.39, bf16[896,2048]{1,0:T(8,128)(2,1)} %bitcast.40), custom_call_target="tpu_custom_call" | custom-call | tf_op jit(solution)/shard_map/pallas_call | solution.py:318
  226.3 0.0 copy-start
  226.3 2.2 fusion.1
  228.5 0.0 copy-done
  228.5 1.3 fusion.3
  (9 shorter events, 0.1 us)
Async XLA Ops:
  25.6 0.7 copy-start.4
  33.0 12.3 %copy-start.3 = (s32[128,2]{0,1:T(2,128)S(1)}, s32[128,2]{0,1:T(2,128)}, u32[]{:S(2)}) copy-start(s32[128,2]{0,1:T(2,128)} %param.23) | copy-start | bytes 3076
  33.0 13.2 %copy-start.5 = (f32[128,2]{0,1:T(2,128)S(1)}, f32[128,2]{0,1:T(2,128)}, u32[]{:S(2)}) copy-start(f32[128,2]{0,1:T(2,128)} %param.24) | copy-start | bytes 3076
  33.0 18.1 %copy-start.1 = (bf16[128,2048]{1,0:T(8,128)(2,1)S(1)}, bf16[128,2048]{1,0:T(8,128)(2,1)}, u32[]{:S(2)}) copy-start(bf16[128,2048]{1,0:T(8,128)(2,1)} %param.21) | copy-start | bytes 1572868
  41.7 9.4 %all-to-all-start = ((bf16[4,128,256]{1,2,0:T(8,128)(2,1)}), bf16[4,128,256]{1,2,0:T(8,128)(2,1)S(1)}, u32[]{:S(2)}, u32[]{:S(2)}) async-start(bf16[4,128,256]{1,2,0:T(8,128)(2,1)} %copy.53), calls=%async_computation | async-start | bytes 524288 | tf_op jit(solution)/shard_map/all_to_all | solution.py:501
  51.1 3.2 %copy-start.2 = (f32[2048]{0:T(1024)S(1)}, f32[2048]{0:T(1024)}, u32[]{:S(2)}) copy-start(f32[2048]{0:T(1024)} %param.22) | copy-start | bytes 24580
  226.3 2.2 copy-start
